TPU v7x, 32 devices: a whole 2x2x4 slice. The times are simulated.
32 devices in a mesh: fs: 4 (over z), rep: 4 (over y, x), tp: 2 (over core).
Axes of the slice: x: 2, y: 2, z: 4, core: 2. Of those that a mesh axis runs over, the one named last changes fastest.
Arguments:
- saved_input: bfloat16 [16384, 2048], P(('fs', 'rep')), may hold values from -500 to 500
- query_cotangent: bfloat16 [16384, 2048], P(('fs', 'rep'), 'tp'), may hold values from -0.014038086 to 0.014038086
- key_cotangent: bfloat16 [16384, 512], P(('fs', 'rep'), 'tp'), may hold values from -0.014038086 to 0.014038086
- query_weight: float32 [2048, 2048], P('fs', 'tp'), may hold values from -45 to 45
- key_weight: float32 [2048, 512], P('fs', 'tp'), may hold values from -45 to 45
- query_moment: float32 [2048, 2048], P('fs', 'tp'), may hold values from -45 to 45
- key_moment: float32 [2048, 512], P('fs', 'tp'), may hold values from -45 to 45
- query_row_root: bfloat16 [2048, 2048], P('fs'), may hold values from -1 to 3, as said below
- key_row_root: bfloat16 [2048, 2048], P('fs'), may hold values from -1 to 3, as said below
- query_head_root: bfloat16 [32, 64, 64], P('tp'), may hold values from -1 to 3, as said below
- key_head_root: bfloat16 [8, 64, 64], P('tp'), may hold values from -1 to 3, as said below
- query_head_stat: float32 [32, 64, 64], P('tp'), may hold values from -26 to 27, as said below
- key_head_stat: float32 [8, 64, 64], P('tp'), may hold values from -26 to 27, as said below
Outputs:
- query_step: float32 [2048, 2048], P('fs', 'tp')
- key_step: float32 [2048, 512], P('fs', 'tp')
- query_next: float32 [2048, 2048], P('fs', 'tp')
- key_next: float32 [2048, 512], P('fs', 'tp')
- query_copy: bfloat16 [2048, 2048], P(None, 'tp')
- key_copy: bfloat16 [2048, 512], P(None, 'tp')
- query_moment_next: float32 [2048, 2048], P('fs', 'tp')
- key_moment_next: float32 [2048, 512], P('fs', 'tp')
- query_stat_next: float32 [32, 64, 64], P('tp')
- key_stat_next: float32 [8, 64, 64], P('tp')
Inputs may be any that keep to these rules, and one draw needn't show every extreme that they name: `query_row_root`: symmetric. `key_row_root`: symmetric. `query_head_root`: each head's matrix is symmetric. `key_head_root`: each head's matrix is symmetric. `query_head_stat`: each head's matrix is symmetric. `key_head_stat`: each head's matrix is symmetric.
All inputs are finite; a program needn't handle non-finite values.
Results may differ from a plain program's by a relative error of at most 0.0018.
The roundings to bfloat16 on the way count: a program that leaves them out, or rounds other values in their place, can miss the bound.
Values may be sent and summed in bfloat16 or wider, within the bound.
A program may use at most 128 MiB of HBM per device.

v0:
```python
import jax
import jax.numpy as jnp
from jax import lax
from jax.sharding import PartitionSpec as P

D = 2048
HEAD_DIM = 64
MOMENT_DECAY = 0.8
STAT_DECAY = 0.5
LEARN_RATE = 0.1
EPSILON = 1e-06


def head_gram(rounded, head_count):
    shaped = rounded.reshape(rounded.shape[0], head_count, HEAD_DIM)
    return jnp.einsum("rhd,rhe->hde", shaped, shaped, preferred_element_type=jnp.float32)


def column_factor(rounded, head_root):
    head_count = head_root.shape[0]
    shaped = rounded.reshape(rounded.shape[0], head_count, HEAD_DIM)
    rightward = jnp.einsum("rhd,hde->rhe", shaped, head_root, preferred_element_type=jnp.float32)
    return rightward.reshape(rounded.shape[0], head_count * HEAD_DIM).astype(jnp.bfloat16)


def shards(
    saved_input,
    query_cotangent,
    key_cotangent,
    query_weight,
    key_weight,
    query_moment,
    key_moment,
    query_row_root,
    key_row_root,
    query_head_root,
    key_head_root,
    query_head_stat,
    key_head_stat,
):
    query_width = query_cotangent.shape[1]
    cotangents = jnp.concatenate([query_cotangent, key_cotangent], axis=1)
    partial_value = lax.psum_scatter(
        lax.dot_general(
            saved_input, cotangents, (((0,), (0,)), ((), ())), preferred_element_type=jnp.float32
        ),
        ("fs", "rep"),
        scatter_dimension=0,
        tiled=True,
    )
    gradient = lax.all_gather(partial_value, "rep", axis=0, tiled=True)
    rounded = gradient.astype(jnp.bfloat16)
    query_rounded = rounded[:, :query_width]
    key_rounded = rounded[:, query_width:]
    query_gram, key_gram = lax.psum(
        (
            head_gram(query_rounded, query_head_root.shape[0]),
            head_gram(key_rounded, key_head_root.shape[0]),
        ),
        "fs",
    )
    query_stat_next = STAT_DECAY * query_head_stat + (1.0 - STAT_DECAY) * query_gram / D
    key_stat_next = STAT_DECAY * key_head_stat + (1.0 - STAT_DECAY) * key_gram / D
    query_right = column_factor(query_rounded, query_head_root)
    key_right = column_factor(key_rounded, key_head_root)
    query_piece = lax.all_gather(query_right, "fs", axis=0, tiled=True)
    key_piece = lax.all_gather(key_right, "fs", axis=0, tiled=True)
    query_pre = jnp.dot(query_row_root, query_piece, preferred_element_type=jnp.float32)
    key_pre = jnp.dot(key_row_root, key_piece, preferred_element_type=jnp.float32)
    query_moment_next = MOMENT_DECAY * query_moment + (1.0 - MOMENT_DECAY) * query_pre
    key_moment_next = MOMENT_DECAY * key_moment + (1.0 - MOMENT_DECAY) * key_pre
    query_wsq, query_msq, key_wsq, key_msq = lax.psum(
        (
            jnp.sum(query_weight * query_weight),
            jnp.sum(query_moment_next * query_moment_next),
            jnp.sum(key_weight * key_weight),
            jnp.sum(key_moment_next * key_moment_next),
        ),
        ("fs", "tp"),
    )
    query_step = (
        LEARN_RATE * (jnp.sqrt(query_wsq) / jnp.sqrt(query_msq + EPSILON)) * query_moment_next
    )
    key_step = LEARN_RATE * (jnp.sqrt(key_wsq) / jnp.sqrt(key_msq + EPSILON)) * key_moment_next
    query_next = query_weight - query_step
    key_next = key_weight - key_step
    query_copy, key_copy = (
        lax.all_gather(query_next.astype(jnp.bfloat16), "fs", axis=0, tiled=True),
        lax.all_gather(key_next.astype(jnp.bfloat16), "fs", axis=0, tiled=True),
    )
    return (
        query_step,
        key_step,
        query_next,
        key_next,
        query_copy,
        key_copy,
        query_moment_next,
        key_moment_next,
        query_stat_next,
        key_stat_next,
    )


def solution(mesh):
    in_specs = (
        P(("fs", "rep"), None),
        P(("fs", "rep"), "tp"),
        P(("fs", "rep"), "tp"),
        P("fs", "tp"),
        P("fs", "tp"),
        P("fs", "tp"),
        P("fs", "tp"),
        P("fs", None),
        P("fs", None),
        P("tp", None, None),
        P("tp", None, None),
        P("tp", None, None),
        P("tp", None, None),
    )
    out_specs = (
        P("fs", "tp"),
        P("fs", "tp"),
        P("fs", "tp"),
        P("fs", "tp"),
        P(None, "tp"),
        P(None, "tp"),
        P("fs", "tp"),
        P("fs", "tp"),
        P("tp", None, None),
        P("tp", None, None),
    )
    return jax.shard_map(shards, mesh=mesh, in_specs=in_specs, out_specs=out_specs, check_vma=False)
```

profile of v0, /device:TPU:0, one launch (start us, length us, event | category | flops | bytes accessed | tf_op | source)
XLA Modules:
  0.0 567.2 jit_solution(7115571609931742830)
XLA Ops:
  7.2 0.0 reduce-scatter.2.cloned.1.call-start
  7.2 10.8 %convolution_bitcast_fusion = f32[2048,1280]{0,1:T(8,128)} fusion(bf16[1024,2048]{1,0:T(8,128)(2,1)} %param.13, bf16[1024,256]{1,0:T(8,128)(2,1)} %param.15, bf16[1024,1024]{1,0:T(8,128)(2,1)} %param.14), kind=kOutput, calls=%fused_computation | convolution fusion | flops 5373952000 | bytes 17301504 | tf_op jit(solution)/shard_map/dot_general | solution.py:44
  18.0 0.0 reduce-scatter.2.cloned.1.call-update
  18.0 0.0 all-gather.6.cloned.1.call-start
  18.1 222.6 %reduce-scatter.2.cloned.1.call-done = f32[128,1280]{0,1:T(8,128)} async-done(((f32[2048,1280]{0,1:T(8,128)}), f32[128,1280]{0,1:T(8,128)}) %reduce-scatter.2.cloned.1.call-update) | async-done | bytes 655376 | tf_op jit(solution)/shard_map/reduce_scatter | solution.py:43
  240.7 0.0 all-gather.6.cloned.1.call-update
  240.7 0.0 all-gather.10.cloned.1.call-start
  240.8 44.8 %all-gather.6.cloned.1.call-done = f32[512,1280]{0,1:T(8,128)} async-done(((f32[128,1280]{0,1:T(8,128)}), f32[512,1280]{0,1:T(8,128)}) %all-gather.6.cloned.1.call-update) | async-done | bytes 2621456 | tf_op jit(solution)/shard_map/all_gather | solution.py:51
  285.6 1.9 convert_element_type.27
  287.5 1.0 copy-done.4
  288.6 1.0 convolution_convert_fusion.1
  289.5 0.0 all-gather.10.cloned.1.call-update
  289.6 0.0 all-gather.8.cloned.1.call-start
  289.6 1.3 slice.8
  290.9 2.4 convolution_convert_fusion
  293.3 0.0 all-gather.8.cloned.1.call-update
  293.3 0.0 all-reduce.4.cloned.1.call-start
  293.4 2.9 copy.23
  296.3 2.1 copy.25
  298.3 2.0 copy.28
  300.4 1.8 multiply_reduce_fusion.3
  302.2 2.7 multiply_reduce_fusion.1
  304.9 0.9 fusion.9
  305.8 1.2 fusion.8
  307.0 0.0 all-reduce.4.cloned.1.call-update
  307.0 0.0 all-gather.14.cloned.1.call-start
  307.0 10.7 %all-gather.10.cloned.1.call-done = bf16[2048,256]{0,1:T(8,128)(2,1)} async-done(((bf16[512,256]{0,1:T(8,128)(2,1)}), bf16[2048,256]{0,1:T(8,128)(2,1)}) %all-gather.10.cloned.1.call-update) | async-done | bytes 1048592 | tf_op jit(solution)/shard_map/all_gather | solution.py:67
  317.7 3.4 multiply_reduce_fusion.2
  321.1 78.7 %all-gather.8.cloned.1.call-done = bf16[2048,1024]{0,1:T(8,128)(2,1)} async-done(((bf16[512,1024]{0,1:T(8,128)(2,1)}), bf16[2048,1024]{0,1:T(8,128)(2,1)}) %all-gather.8.cloned.1.call-update) | async-done | bytes 4194320 | tf_op jit(solution)/shard_map/all_gather | solution.py:66
  399.8 7.2 %multiply_reduce_fusion = (f32[]{:T(128)}, f32[512,1024]{0,1:T(8,128)}) fusion(bf16[2048,1024]{0,1:T(8,128)(2,1)} %all-gather.8.cloned.1.call-done, bf16[512,2048]{1,0:T(8,128)(2,1)S(1)} %copy-done, f32[512,1024]{0,1:T(8,128)} %copy.23), kind=kOutput, calls=%fused_computation.5 | convolution fusion | flops 2150105088 | bytes 10485764 | tf_op jit(solution)/shard_map/dot_general | solution.py:68
  407.1 14.9 %all-reduce = (f32[]{:T(128)}, f32[]{:T(128)}, f32[]{:T(128)}, f32[]{:T(128)}) all-reduce(f32[]{:T(128)} %multiply_reduce_fusion.1, f32[]{:T(128)} %get-tuple-element.32, f32[]{:T(128)} %multiply_reduce_fusion.3, f32[]{:T(128)} %get-tuple-element.34), channel_id=1, replica_groups=mesh['fs'=4,'rep'=4,'tp'=2] {'fs','tp'}, use_global_device_ids=true, to_apply=%region_1.0 | all-reduce | flops 4 | bytes 32 | tf_op jit(solution)/shard_map/psum | solution.py:72
  423.4 2.1 fusion.6
  425.5 0.0 all-gather.12.cloned.1.call-start
  425.5 3.0 copy.27
  429.9 4.7 fusion.7
  434.6 8.0 %all-reduce.4.cloned.1.call-done = (f32[16,64,64]{2,1,0:T(8,128)}, f32[4,64,64]{2,1,0:T(8,128)}) async-done(((f32[16,64,64]{2,1,0:T(8,128)}, f32[4,64,64]{2,1,0:T(8,128)}), (f32[16,64,64]{2,1,0:T(8,128)}, f32[4,64,64]{2,1,0:T(8,128)})) %all-reduce.4.cloned.1.call-update) | async-done | bytes 327696 | tf_op jit(solution)/shard_map/psum | solution.py:55
  442.6 1.6 multiply_add_fusion.1
  444.2 2.1 multiply_add_fusion
  446.3 1.0 copy.36
  447.3 1.8 copy.35
  449.1 3.0 copy.29
  452.1 1.0 copy.30
  453.1 1.8 copy.31
  454.9 1.0 copy.32
  455.9 16.1 %all-gather.14.cloned.1.call-done = bf16[2048,256]{0,1:T(8,128)(2,1)} async-done(((bf16[512,256]{0,1:T(8,128)(2,1)}), bf16[2048,256]{0,1:T(8,128)(2,1)}) %all-gather.14.cloned.1.call-update) | async-done | bytes 1048592 | tf_op jit(solution)/shard_map/all_gather | solution.py:89
  472.1 2.3 copy.34
  474.3 79.5 %all-gather.12.cloned.1.call-done = bf16[2048,1024]{0,1:T(8,128)(2,1)} async-done(((bf16[512,1024]{0,1:T(8,128)(2,1)}), bf16[2048,1024]{0,1:T(8,128)(2,1)}) %all-gather.12.cloned.1.call-update) | async-done | bytes 4194320 | tf_op jit(solution)/shard_map/all_gather | solution.py:88
  553.8 6.5 %copy.33 = bf16[2048,1024]{1,0:T(8,128)(2,1)} copy(bf16[2048,1024]{0,1:T(8,128)(2,1)} %all-gather.12.cloned.1.call-done) | data formatting | bytes 8388608
  (18 shorter events, 0.1 us)
Async XLA Ops:
  7.2 392.7 %copy-start = (bf16[512,2048]{1,0:T(8,128)(2,1)S(1)}, bf16[512,2048]{1,0:T(8,128)(2,1)}, u32[]{:S(2)}) copy-start(bf16[512,2048]{1,0:T(8,128)(2,1)} %param.20) | copy-start | bytes 6291460
  7.2 233.5 %reduce-scatter.2.cloned.1.call-start = ((), (), s32[]{:S(2)}) async-start(), calls=%async_computation.1 | async-start | bytes 11141120 | tf_op jit(solution)/shard_map/reduce_scatter | solution.py:43
  18.0 267.5 %all-gather.6.cloned.1.call-start = ((), (), s32[]{:S(2)}) async-start(), calls=%async_computation.2 | async-start | bytes 3276800 | tf_op jit(solution)/shard_map/all_gather | solution.py:51
  240.7 47.8 %copy-start.7 = (bf16[4,64,64]{2,1,0:T(8,128)(2,1)S(1)}, bf16[4,64,64]{2,1,0:T(8,128)(2,1)}, u32[]{:S(2)}) copy-start(bf16[4,64,64]{2,1,0:T(8,128)(2,1)} %param.23) | copy-start | bytes 98308
  240.7 77.0 %all-gather.10.cloned.1.call-start = ((), (), s32[]{:S(2)}) async-start(), calls=%async_computation.4 | async-start | bytes 1310720 | tf_op jit(solution)/shard_map/all_gather | solution.py:67
  287.5 1.1 copy-start.4
  289.6 110.3 %all-gather.8.cloned.1.call-start = ((), (), s32[]{:S(2)}) async-start(), calls=%async_computation.3 | async-start | bytes 5242880 | tf_op jit(solution)/shard_map/all_gather | solution.py:66
  293.3 149.3 %all-reduce.4.cloned.1.call-start = ((), (), s32[]{:S(2)}) async-start(), calls=%async_computation.7 | async-start | bytes 1310720 | tf_op jit(solution)/shard_map/psum | solution.py:55
  307.0 165.1 %all-gather.14.cloned.1.call-start = ((), (), s32[]{:S(2)}) async-start(), calls=%async_computation.6 | async-start | bytes 1310720 | tf_op jit(solution)/shard_map/all_gather | solution.py:89
  425.4 4.5 copy-start.2
  425.5 128.3 %all-gather.12.cloned.1.call-start = ((), (), s32[]{:S(2)}) async-start(), calls=%async_computation.5 | async-start | bytes 5242880 | tf_op jit(solution)/shard_map/all_gather | solution.py:88
  429.9 12.7 %copy-start.6 = (f32[4,64,64]{2,1,0:T(8,128)S(1)}, f32[4,64,64]{2,1,0:T(8,128)}, u32[]{:S(2)}) copy-start(f32[4,64,64]{2,1,0:T(8,128)} %param.25) | copy-start | bytes 196612
  449.1 3.0 copy-start.5
  449.1 4.0 copy-start.3
  553.8 6.5 %copy-start.1 = (bf16[512,2048]{1,0:T(8,128)(2,1)S(1)}, bf16[512,2048]{1,0:T(8,128)(2,1)}, u32[]{:S(2)}) copy-start(bf16[512,2048]{1,0:T(8,128)(2,1)} %param.20) | copy-start | bytes 6291460
Sparse Core Ops, SparseCore 0:
  18.1 222.5 reduce-scatter.1
  242.5 42.9 all-gather.5
  289.7 27.9 all-gather.9
  319.7 80.1 all-gather.7
  403.3 39.3 all-reduce.3
  444.6 27.3 all-gather.13
  473.6 80.1 all-gather.11
where the time goes:
time: 568 us; the launch traced here: 567 us
  waiting for transfers between devices  460 us (81%)
  local copies, waits for them, and re-layouts  30.8 us (5%)
  matrix products  26.8 us (5%)
  between operations  17 us (3%)
  other arithmetic  16.8 us (3%)
  blocking collectives  14.9 us (3%)
    reduce_scatter x1, waiting for transfers between devices, shards(): lax.psum_scatter(lax.dot_general(saved_input, cotangents, (((0,), (0,)),...  223 us
    all_gather x1, waiting for transfers between devices, shards(): lax.all_gather(query_next.astype(jnp.bfloat16), 'fs', axis=0, tiled=True)  79.5 us
    all_gather x1, waiting for transfers between devices, shards(): query_piece = lax.all_gather(query_right, 'fs', axis=0, tiled=True)  78.7 us
    all_gather x1, waiting for transfers between devices, shards(): gradient = lax.all_gather(partial_value, 'rep', axis=0, tiled=True)  44.8 us
    unnamed x28, local copies, waits for them, and re-layouts  29.5 us
    all_gather x1, waiting for transfers between devices, shards(): lax.all_gather(key_next.astype(jnp.bfloat16), 'fs', axis=0, tiled=True)  16.1 us
    psum x1, blocking collectives, shards(): lax.psum((jnp.sum(query_weight * query_weight), jnp.sum(query_moment_next...  14.9 us
  transfers between devices with their start and end apart: 7, of which 7 were waited for; matrix products, arithmetic and copies ran while one was open for 9% of the time, Pallas kernels for 0%

commit v1 on v0

--- a/solution.py
+++ b/solution.py
@@ -63,7 +63,12 @@
     key_stat_next = STAT_DECAY * key_head_stat + (1.0 - STAT_DECAY) * key_gram / D
     query_right = column_factor(query_rounded, query_head_root)
     key_right = column_factor(key_rounded, key_head_root)
-    query_piece = lax.all_gather(query_right, "fs", axis=0, tiled=True)
+    ring = [query_right]
+    for hop in range(3):
+        ring.append(lax.ppermute(ring[-1], "fs", [(dev, (dev + 1) % 4) for dev in range(4)]))
+    query_piece = jnp.roll(
+        jnp.concatenate(ring[::-1], axis=0), (lax.axis_index("fs") + 1) * ring[0].shape[0], axis=0
+    )
     key_piece = lax.all_gather(key_right, "fs", axis=0, tiled=True)
     query_pre = jnp.dot(query_row_root, query_piece, preferred_element_type=jnp.float32)
     key_pre = jnp.dot(key_row_root, key_piece, preferred_element_type=jnp.float32)

time: 568 us -> 543 us (0.956)
  waiting for transfers between devices: 460 us -> 430 us
  local copies, waits for them, and re-layouts: 30.8 us -> 40.3 us
    ppermute x0 -> x3, waiting for transfers between devices: none -> 82.9 us  [shards(): lax.ppermute(ring[-1], 'fs', [(dev, (dev + 1) % 4) for dev in range(4)])]
    all_gather x1 -> x0, waiting for transfers between devices: 78.7 us -> none  [shards(): query_piece = lax.all_gather(query_right, 'fs', axis=0, tiled=True)]
    all_gather x1, waiting for transfers between devices: 16.1 us -> 0.22 us  [shards(): lax.all_gather(key_next.astype(jnp.bfloat16), 'fs', axis=0, tiled=True)]
    all_gather x1, waiting for transfers between devices: 10.7 us -> 0.02 us  [shards(): key_piece = lax.all_gather(key_right, 'fs', axis=0, tiled=True)]
    unnamed x28 -> x41, local copies, waits for them, and re-layouts: 29.5 us -> 40.1 us
    psum x1, waiting for transfers between devices: 7.98 us -> 0.02 us  [shards(): lax.psum((head_gram(query_rounded, query_head_root.shape[0]), head_gram(k...]
  transfers between devices with their start and end apart: 7 -> 9, of which waited for: 7 -> 7; matrix products, arithmetic and copies ran while one was open for 9% -> 11% of each run, Pallas kernels for 0% -> 0%
where the time goes in v1:
time: 543 us; the launch traced here: 542 us
  waiting for transfers between devices  430 us (79%)
  local copies, waits for them, and re-layouts  40.3 us (7%)
  matrix products  22.1 us (4%)
  between operations  17.1 us (3%)
  other arithmetic  16.6 us (3%)
  blocking collectives  14.3 us (3%)
    reduce_scatter x1, waiting for transfers between devices, shards(): lax.psum_scatter(lax.dot_general(saved_input, cotangents, (((0,), (0,)),...  223 us
    ppermute x3, waiting for transfers between devices, shards(): lax.ppermute(ring[-1], 'fs', [(dev, (dev + 1) % 4) for dev in range(4)])  82.9 us
    all_gather x1, waiting for transfers between devices, shards(): lax.all_gather(query_next.astype(jnp.bfloat16), 'fs', axis=0, tiled=True)  79.3 us
    all_gather x1, waiting for transfers between devices, shards(): gradient = lax.all_gather(partial_value, 'rep', axis=0, tiled=True)  44.8 us
    unnamed x41, local copies, waits for them, and re-layouts  40.1 us
    psum x1, blocking collectives, shards(): lax.psum((jnp.sum(query_weight * query_weight), jnp.sum(query_moment_next...  14.3 us
  transfers between devices with their start and end apart: 9, of which 7 were waited for; matrix products, arithmetic and copies ran while one was open for 11% of the time, Pallas kernels for 0%

profile of v1, /device:TPU:0, one launch (start us, length us, event | category | flops | bytes accessed | tf_op | source)
XLA Modules:
  0.0 542.3 jit_solution(5506679058466528549)
XLA Ops:
  7.2 10.8 %convolution_bitcast_fusion = f32[2048,1280]{0,1:T(8,128)} fusion(bf16[1024,2048]{1,0:T(8,128)(2,1)} %param.13, bf16[1024,256]{1,0:T(8,128)(2,1)} %param.15, bf16[1024,1024]{1,0:T(8,128)(2,1)} %param.14), kind=kOutput, calls=%fused_computation | convolution fusion | flops 5373952000 | bytes 17301504 | tf_op jit(solution)/shard_map/dot_general | solution.py:44
  18.1 222.6 %reduce-scatter.2.cloned.1.call-done = f32[128,1280]{0,1:T(8,128)} async-done(((f32[2048,1280]{0,1:T(8,128)}), f32[128,1280]{0,1:T(8,128)}) %reduce-scatter.2.cloned.1.call-update) | async-done | bytes 655376 | tf_op jit(solution)/shard_map/reduce_scatter | solution.py:43
  240.8 44.8 %all-gather.5.cloned.1.call-done = f32[512,1280]{0,1:T(8,128)} async-done(((f32[128,1280]{0,1:T(8,128)}), f32[512,1280]{0,1:T(8,128)}) %all-gather.5.cloned.1.call-update) | async-done | bytes 2621456 | tf_op jit(solution)/shard_map/all_gather | solution.py:51
  285.6 1.9 convert_element_type.27
  287.5 0.1 slice.8
  287.6 0.5 convolution_convert_fusion
  288.1 1.0 copy-done.1
  289.1 1.5 collective-permute-start
  290.6 25.1 %collective-permute-done = bf16[512,1024]{0,1:T(8,128)(2,1)} collective-permute-done((bf16[512,1024]{0,1:T(8,128)(2,1)S(1)}, bf16[512,1024]{0,1:T(8,128)(2,1)}, u32[]{:S(2)}, u32[]{:S(2)}) %collective-permute-start) | collective-permute-done | bytes 1048608 | tf_op jit(solution)/shard_map/ppermute | solution.py:68
  315.7 1.0 convolution_convert_fusion.1
  316.8 2.9 copy.23
  319.7 2.0 copy.25
  321.7 2.0 copy.28
  323.7 1.8 multiply_reduce_fusion.3
  325.5 30.5 %collective-permute-done.1 = bf16[512,1024]{0,1:T(8,128)(2,1)} collective-permute-done((bf16[512,1024]{0,1:T(8,128)(2,1)}, bf16[512,1024]{0,1:T(8,128)(2,1)}, u32[]{:S(2)}, u32[]{:S(2)}) %collective-permute-start.1) | collective-permute-done | bytes 1048608 | tf_op jit(solution)/shard_map/ppermute | solution.py:68
  356.1 2.7 multiply_reduce_fusion.1
  358.8 0.9 fusion.14
  359.7 1.2 fusion.13
  360.9 0.0 all-gather.11.cloned.1.call-start
  361.0 3.4 multiply_reduce_fusion.2
  364.4 27.2 %collective-permute-done.2 = bf16[512,1024]{0,1:T(8,128)(2,1)} collective-permute-done((bf16[512,1024]{0,1:T(8,128)(2,1)}, bf16[512,1024]{0,1:T(8,128)(2,1)}, u32[]{:S(2)}, u32[]{:S(2)}) %collective-permute-start.2) | collective-permute-done | bytes 1048608 | tf_op jit(solution)/shard_map/ppermute | solution.py:68
  391.6 1.4 constant_dynamic-update-slice_fusion.7
  393.0 1.5 constant_dynamic-update-slice_fusion.6
  394.5 1.4 constant_dynamic-update-slice_fusion.5
  395.9 0.1 constant_dynamic-update-slice_fusion.4
  396.1 1.4 constant_dynamic-update-slice_fusion.3
  397.5 1.4 constant_dynamic-update-slice_fusion.2
  398.9 1.5 constant_dynamic-update-slice_fusion.1
  400.4 0.2 constant_dynamic-update-slice_fusion
  400.6 0.2 copy-done.6
  400.8 4.4 multiply_reduce_fusion
  405.2 14.3 %all-reduce = (f32[]{:T(128)}, f32[]{:T(128)}, f32[]{:T(128)}, f32[]{:T(128)}) all-reduce(f32[]{:T(128)} %multiply_reduce_fusion.1, f32[]{:T(128)} %get-tuple-element.32, f32[]{:T(128)} %multiply_reduce_fusion.3, f32[]{:T(128)} %get-tuple-element.34), channel_id=1, replica_groups=mesh['fs'=4,'rep'=4,'tp'=2] {'fs','tp'}, use_global_device_ids=true, to_apply=%region_1.0 | all-reduce | flops 4 | bytes 32 | tf_op jit(solution)/shard_map/psum | solution.py:77
  420.9 1.2 fusion.11
  422.1 0.2 all-gather.9.cloned.1.call-start
  422.3 2.9 copy.27
  426.6 5.4 %fusion.12 = (bf16[512,1024]{0,1:T(8,128)(2,1)}, f32[512,1024]{0,1:T(8,128)}, f32[512,1024]{0,1:T(8,128)}) fusion(f32[512,1024]{0,1:T(8,128)} %copy.27, f32[512,1024]{0,1:T(8,128)} %get-tuple-element.33, f32[]{:T(128)S(6)} %mul.79), kind=kLoop, calls=%fused_computation.31 | loop fusion | flops 1572864 | bytes 9437188 | tf_op jit(solution)/shard_map/convert_element_type | solution.py:93
  432.1 1.6 multiply_add_fusion.1
  433.7 1.9 multiply_add_fusion
  435.6 1.0 copy.36
  436.6 2.9 copy.35
  439.5 1.0 copy.30
  440.5 1.0 copy.32
  441.5 2.9 copy.29
  444.4 2.9 copy.31
  447.3 0.2 all-gather.11.cloned.1.call-done
  447.5 2.3 copy.34
  449.7 79.3 %all-gather.9.cloned.1.call-done = bf16[2048,1024]{0,1:T(8,128)(2,1)} async-done(((bf16[512,1024]{0,1:T(8,128)(2,1)}), bf16[2048,1024]{0,1:T(8,128)(2,1)}) %all-gather.9.cloned.1.call-update) | async-done | bytes 4194320 | tf_op jit(solution)/shard_map/all_gather | solution.py:93
  529.1 6.4 %copy.33 = bf16[2048,1024]{1,0:T(8,128)(2,1)} copy(bf16[2048,1024]{0,1:T(8,128)(2,1)} %all-gather.9.cloned.1.call-done) | data formatting | bytes 8388608
  (35 shorter events, 0.4 us)
Async XLA Ops:
  7.2 393.4 %copy-start = (bf16[512,2048]{1,0:T(8,128)(2,1)S(1)}, bf16[512,2048]{1,0:T(8,128)(2,1)}, u32[]{:S(2)}) copy-start(bf16[512,2048]{1,0:T(8,128)(2,1)} %param.20) | copy-start | bytes 6291460
  7.2 233.6 %reduce-scatter.2.cloned.1.call-start = ((), (), s32[]{:S(2)}) async-start(), calls=%async_computation.1 | async-start | bytes 11141120 | tf_op jit(solution)/shard_map/reduce_scatter | solution.py:43
  18.1 267.5 %all-gather.5.cloned.1.call-start = ((), (), s32[]{:S(2)}) async-start(), calls=%async_computation.2 | async-start | bytes 3276800 | tf_op jit(solution)/shard_map/all_gather | solution.py:51
  240.8 46.8 %copy-start.8 = (bf16[16,64,64]{2,1,0:T(8,128)(2,1)S(1)}, bf16[16,64,64]{2,1,0:T(8,128)(2,1)}, u32[]{:S(2)}) copy-start(bf16[16,64,64]{2,1,0:T(8,128)(2,1)} %param.22) | copy-start | bytes 393220
  240.8 120.2 %all-gather.7.cloned.1.call-start = ((), (), s32[]{:S(2)}) async-start(), calls=%async_computation.3 | async-start | bytes 1310720 | tf_op jit(solution)/shard_map/all_gather | solution.py:72
  287.5 28.2 %copy-start.10 = (bf16[4,64,64]{2,1,0:T(8,128)(2,1)S(1)}, bf16[4,64,64]{2,1,0:T(8,128)(2,1)}, u32[]{:S(2)}) copy-start(bf16[4,64,64]{2,1,0:T(8,128)(2,1)} %param.23) | copy-start | bytes 98308
  288.1 1.0 copy-start.1
  289.1 26.6 %collective-permute-start = (bf16[512,1024]{0,1:T(8,128)(2,1)S(1)}, bf16[512,1024]{0,1:T(8,128)(2,1)}, u32[]{:S(2)}, u32[]{:S(2)}) collective-permute-start(bf16[512,1024]{0,1:T(8,128)(2,1)S(1)} %bitcast.30), channel_id=1, source_target_pairs={{0,8},{8,16},{16,24},{24,0},{1,9},{9,17},{17,25},{25,1},{2,10},{10... | collective-permute-start | bytes 3145736 | tf_op jit(solution)/shard_map/ppermute | solution.py:68
  315.7 40.4 %collective-permute-start.1 = (bf16[512,1024]{0,1:T(8,128)(2,1)}, bf16[512,1024]{0,1:T(8,128)(2,1)}, u32[]{:S(2)}, u32[]{:S(2)}) collective-permute-start(bf16[512,1024]{0,1:T(8,128)(2,1)} %collective-permute-done), channel_id=1, source_target_pairs={{0,8},{8,16},{16,24},{24,0},{1,9},{9,17},{17,25},{25,1},{2,10},{10... | collective-permute-start | bytes 3145736 | tf_op jit(solution)/shard_map/ppermute | solution.py:68
  316.7 115.3 %all-reduce.4.cloned.1.call-start = ((), (), s32[]{:S(2)}) async-start(), calls=%async_computation.6 | async-start | bytes 1310720 | tf_op jit(solution)/shard_map/psum | solution.py:55
  356.1 35.5 %collective-permute-start.2 = (bf16[512,1024]{0,1:T(8,128)(2,1)}, bf16[512,1024]{0,1:T(8,128)(2,1)}, u32[]{:S(2)}, u32[]{:S(2)}) collective-permute-start(bf16[512,1024]{0,1:T(8,128)(2,1)} %collective-permute-done.1), channel_id=1, source_target_pairs={{0,8},{8,16},{16,24},{24,0},{1,9},{9,17},{17,25},{25,1},{2,10},{10... | collective-permute-start | bytes 3145736 | tf_op jit(solution)/shard_map/ppermute | solution.py:68
  360.9 86.6 %all-gather.11.cloned.1.call-start = ((), (), s32[]{:S(2)}) async-start(), calls=%async_computation.5 | async-start | bytes 1310720 | tf_op jit(solution)/shard_map/all_gather | solution.py:94
  393.0 2.9 copy-start.2
  398.9 1.9 copy-start.6
  400.8 20.1 %copy-start.3 = (f32[512,256]{0,1:T(8,128)S(1)}, f32[512,256]{0,1:T(8,128)}, u32[]{:S(2)}) copy-start(f32[512,256]{0,1:T(8,128)} %copy.28) | copy-start | bytes 1572868
  422.1 107.0 %all-gather.9.cloned.1.call-start = ((), (), s32[]{:S(2)}) async-start(), calls=%async_computation.4 | async-start | bytes 5242880 | tf_op jit(solution)/shard_map/all_gather | solution.py:93
  426.5 5.5 %copy-start.9 = (f32[4,64,64]{2,1,0:T(8,128)S(1)}, f32[4,64,64]{2,1,0:T(8,128)}, u32[]{:S(2)}) copy-start(f32[4,64,64]{2,1,0:T(8,128)} %param.25) | copy-start | bytes 196612
  426.6 7.1 %copy-start.7 = (f32[16,64,64]{2,1,0:T(8,128)S(1)}, f32[16,64,64]{2,1,0:T(8,128)}, u32[]{:S(2)}) copy-start(f32[16,64,64]{2,1,0:T(8,128)} %param.24) | copy-start | bytes 786436
  435.6 3.9 copy-start.5
  436.6 3.9 copy-start.4
Sparse Core Ops, SparseCore 0:
  18.2 222.5 reduce-scatter.1
  242.6 42.9 all-gather.4
  316.8 42.4 all-gather.6
  362.8 47.3 all-reduce.3
  422.2 25.2 all-gather.10
  448.9 80.1 all-gather.8
